TPU v7x, 256 devices: a whole 4x4x8 slice. The times are simulated.
256 devices in a mesh: sp: 32 (over z, x), tp: 8 (over y, core).
Axes of the slice: x: 4, y: 4, z: 8, core: 2. Of those that a mesh axis runs over, the one named last changes fastest.
Arguments:
- latents: bfloat16 [16384, 2048], P(('sp', 'tp')), may hold values from -6 to 6
- context: bfloat16 [512, 2048], P('sp'), may hold values from -6 to 6
- cond: float32 [2048], P('sp'), may hold values from -6 to 6
- ctx_cond: float32 [2048], P('sp'), may hold values from -6 to 6
- mod_weight: float32 [2048, 6144], P('sp', 'tp'), may hold values from -0.125 to 0.125
- query_weight: bfloat16 [2048, 2048], P(None, 'tp'), may hold values from -1 to 1, as said below
- key_matrix: bfloat16 [2048, 1024], P(None, 'tp'), may hold values from -1 to 1, as said below
- value_matrix: bfloat16 [2048, 1024], P(None, 'tp'), may hold values from -0.125 to 0.125
- out_weight: bfloat16 [2048, 2048], P('tp'), may hold values from -0.125 to 0.125
- query_gain: float32 [128], replicated, may hold values from 0.7 to 7
- key_gain: float32 [128], replicated, may hold values from 0.7 to 7
Outputs:
- updated: bfloat16 [16384, 2048], P(('sp', 'tp'))
Inputs may be any that keep to these rules, and one draw needn't show every extreme that they name: `query_weight`: entries of order 2048 to the power -1/2. `key_matrix`: entries of order 2048 to the power -1/2.
All inputs are finite; a program needn't handle non-finite values.
Results may differ from a plain program's by a relative error of at most 0.0085.
The roundings to bfloat16 on the way count: a program that leaves them out, or rounds other values in their place, can miss the bound.
Values may be sent and summed in bfloat16 or wider, within the bound.
No kernel may reach another device: no remote copies, remote signals or barrier semaphores. Data moves between devices by JAX's collectives and lax.ppermute only.
A program may use at most 128 MiB of HBM per device.

v0:
```python
import math
import jax
import jax.numpy as jnp
from jax import lax
from jax.sharding import Mesh
from jax.sharding import PartitionSpec as P

GRID_W = 64
SP = ("sp_0", "sp_1")
SP_TP = ("sp_0", "sp_1", "tp")
NORM_EPS = 1e-06
ROPE_BASE = 10000.0


def over_axes(value, axes):
    for axis in axes:
        value = lax.psum(value, axis)
    return value


def side_by_side(arrays, axis, dim, along):
    both = jnp.concatenate(arrays, axis=along)
    filled, at, done = (lax.all_gather(both, axis, axis=dim, tiled=True), 0, [])
    for a in arrays:
        done.append(lax.slice_in_dim(filled, at, at + a.shape[along], axis=along))
        at += a.shape[along]
    return tuple(done)


def normalize(latent_value_rows):
    return latent_value_rows * lax.rsqrt(
        jnp.mean(latent_value_rows * latent_value_rows, axis=-1, keepdims=True) + NORM_EPS
    )


def rotate(latent_value_rows, positions):
    quarter = latent_value_rows.shape[-1] // 2
    inv_freq = ROPE_BASE ** (-jnp.arange(quarter, dtype=jnp.float32) / quarter)
    angles = positions.astype(jnp.float32)[:, None] * inv_freq[None, :]
    cos_table = jnp.cos(angles)[:, None, :]
    sin_table = jnp.sin(angles)[:, None, :]
    first, second = (latent_value_rows[..., :quarter], latent_value_rows[..., quarter:])
    return jnp.concatenate(
        [first * cos_table - second * sin_table, second * cos_table + first * sin_table], axis=-1
    )


def axial(latent_value_rows, positions):
    half_dim = latent_value_rows.shape[-1] // 2
    return jnp.concatenate(
        [
            rotate(latent_value_rows[..., :half_dim], positions // GRID_W),
            rotate(latent_value_rows[..., half_dim:], positions % GRID_W),
        ],
        axis=-1,
    )


def modulate(latent_value_rows, mod_row):
    model_width = latent_value_rows.shape[-1]
    shift_vec = mod_row[:model_width]
    scale_vec = mod_row[model_width : 2 * model_width]
    return (
        normalize(latent_value_rows.astype(jnp.float32)) * (1.0 + scale_vec) + shift_vec
    ).astype(jnp.bfloat16)


def body(
    latents,
    context,
    cond,
    ctx_cond,
    mod_weight,
    query_weight,
    key_matrix,
    value_matrix,
    out_weight,
    query_gain,
    key_gain,
):
    model_width = latents.shape[1]
    head_dim = query_gain.shape[0]
    sp_count = lax.axis_size(SP)
    partials = jnp.dot(
        jax.nn.silu(jnp.stack([cond, ctx_cond])), mod_weight, precision=lax.Precision.HIGHEST
    )
    summed = over_axes(partials, SP)
    modulation = lax.all_gather(summed, "tp", axis=1, tiled=True)
    gate_vec = modulation[0, 2 * model_width :]
    normalised_rows = modulate(latents, modulation[0])
    prefix_normalised = modulate(context, modulation[1])
    query_cols = query_weight.shape[1]
    key_cols = key_matrix.shape[1]
    piece = lax.all_gather(normalised_rows, "tp", axis=0, tiled=True)
    projected = jnp.concatenate(
        [
            jnp.dot(piece, query_weight, preferred_element_type=jnp.float32),
            jnp.dot(piece, key_matrix, preferred_element_type=jnp.float32),
            jnp.dot(piece, value_matrix, preferred_element_type=jnp.float32),
        ],
        axis=1,
    )
    row_count = projected.shape[0]
    positions = lax.axis_index(SP) * row_count + jnp.arange(row_count, dtype=jnp.int32)
    query_heads = projected[:, :query_cols].reshape(row_count, -1, head_dim)
    query_heads = axial(normalize(query_heads) * query_gain, positions).astype(jnp.bfloat16)
    key_heads = projected[:, query_cols : query_cols + key_cols].reshape(row_count, -1, head_dim)
    key_heads = axial(normalize(key_heads) * key_gain, positions).astype(jnp.bfloat16)
    value_heads = (
        projected[:, query_cols + key_cols :].reshape(row_count, -1, head_dim).astype(jnp.bfloat16)
    )
    key_part = jnp.dot(prefix_normalised, key_matrix, preferred_element_type=jnp.float32).reshape(
        prefix_normalised.shape[0], -1, head_dim
    )
    value_part = jnp.dot(
        prefix_normalised, value_matrix, preferred_element_type=jnp.float32
    ).reshape(prefix_normalised.shape[0], -1, head_dim)
    local_keys = (normalize(key_part) * key_gain).astype(jnp.bfloat16)
    local_values = value_part.astype(jnp.bfloat16)
    prefix_keys, prefix_values = side_by_side((local_keys, local_values), SP, 0, 1)
    kv_local = key_heads.shape[1]
    group_size = query_heads.shape[1] // kv_local
    grouped = query_heads.reshape(row_count, kv_local, group_size, head_dim).transpose(1, 2, 0, 3)
    grouped = grouped.reshape(kv_local, group_size * row_count, head_dim)
    inv_root = head_dim ** (-0.5)
    lift = math.log(sp_count * row_count / (2.0 * prefix_keys.shape[0]))
    ctx_scores = (
        jnp.einsum("hqd,khd->hqk", grouped, prefix_keys, preferred_element_type=jnp.float32)
        * inv_root
        + lift
    )
    top_init = jnp.max(ctx_scores, axis=-1)
    ctx_weights = jnp.exp(ctx_scores - top_init[..., None])
    initial = (
        top_init,
        jnp.sum(ctx_weights, axis=-1),
        jnp.einsum(
            "hqk,khd->hqd",
            ctx_weights.astype(jnp.bfloat16),
            prefix_values,
            preferred_element_type=jnp.float32,
        ),
    )

    def update(state_now, key_block, value_block):
        top_old, total_old, acc_old = state_now
        scores = (
            jnp.einsum("hqd,khd->hqk", grouped, key_block, preferred_element_type=jnp.float32)
            * inv_root
        )
        top_new = jnp.maximum(top_old, jnp.max(scores, axis=-1))
        factor = jnp.exp(top_old - top_new)
        weights_now = jnp.exp(scores - top_new[..., None])
        acc_new = acc_old * factor[..., None] + jnp.einsum(
            "hqk,khd->hqd",
            weights_now.astype(jnp.bfloat16),
            value_block,
            preferred_element_type=jnp.float32,
        )
        return (top_new, total_old * factor + jnp.sum(weights_now, axis=-1), acc_new)

    key_piece, value_piece = side_by_side((key_heads, value_heads), SP, 0, 1)
    key_count = key_piece.shape[0]
    rows_per_block = math.gcd(key_count, 2048)
    block_count = key_count // rows_per_block
    key_blocks = key_piece.reshape(block_count, rows_per_block, kv_local, head_dim)
    value_blocks = value_piece.reshape(block_count, rows_per_block, kv_local, head_dim)

    def one_step(state_in, blocks_in):
        return (update(state_in, blocks_in[0], blocks_in[1]), None)

    state_out, _ = lax.scan(one_step, initial, (key_blocks, value_blocks))
    top_fin, total_fin, acc_fin = state_out
    attended = (acc_fin / total_fin[..., None]).astype(jnp.bfloat16)
    attended = (
        attended.reshape(kv_local, group_size, row_count, head_dim)
        .transpose(2, 0, 1, 3)
        .reshape(row_count, -1)
    )
    exchanged = lax.all_to_all(attended, "tp", split_axis=0, concat_axis=1, tiled=True)
    mixed_rows = jnp.dot(
        exchanged,
        lax.all_gather(out_weight, "tp", axis=0, tiled=True),
        preferred_element_type=jnp.float32,
    )
    return (latents.astype(jnp.float32) + gate_vec * normalize(mixed_rows)).astype(jnp.bfloat16)


def solution(mesh):
    torus = Mesh(mesh.devices.reshape(8, 4, mesh.shape["tp"]), ("sp_0", "sp_1", "tp"))
    placed = (
        P(SP_TP, None),
        P(SP, None),
        P(SP),
        P(SP),
        P(SP, "tp"),
        P(None, "tp"),
        P(None, "tp"),
        P(None, "tp"),
        P("tp", None),
        P(),
        P(),
    )
    return jax.shard_map(
        body, mesh=torus, in_specs=placed, out_specs=P(SP_TP, None), check_vma=False
    )
```

profile of v0, /device:TPU:1, one launch (start us, length us, event | category | flops | bytes accessed | tf_op | source)
XLA Modules:
  0.0 285.0 jit_solution(6609689054624795851)
XLA Ops:
  7.8 17.5 %psum.14 = f32[2,768]{1,0:T(2,128)S(1)} all-reduce(f32[2,768]{1,0:T(2,128)S(1)} %fusion.67), channel_id=1, replica_groups=mesh['sp_0'=8,'sp_1'=4,'tp'=8] {'sp_0'}, use_global_device_ids=true, to_apply=%region_0.1 | all-reduce | flops 1536 | bytes 12288 | tf_op jit(solution)/shard_map/psum | solution.py:17
  25.3 8.6 %psum.15 = f32[2,768]{1,0:T(2,128)S(1)} all-reduce(f32[2,768]{1,0:T(2,128)S(1)} %psum.14), channel_id=1, replica_groups=mesh['sp_0'=8,'sp_1'=4,'tp'=8] {'sp_1'}, use_global_device_ids=true, to_apply=%region_1.2 | all-reduce | flops 1536 | bytes 12288 | tf_op jit(solution)/shard_map/psum | solution.py:17
  33.9 19.5 %all_gather.15 = f32[2,6144]{1,0:T(2,128)S(1)} all-gather(f32[2,768]{1,0:T(2,128)S(1)} %psum.15), channel_id=1, replica_groups=mesh['sp_0'=8,'sp_1'=4,'tp'=8] {'tp'}, dimensions={1}, use_global_device_ids=true | all-gather | bytes 55296 | tf_op jit(solution)/shard_map/all_gather | solution.py:88
  56.5 23.1 %all-gather.4.cloned.1.call-done = bf16[512,2048]{1,0:T(8,128)(2,1)} async-done(((bf16[64,2048]{1,0:T(8,128)(2,1)}), bf16[512,2048]{1,0:T(8,128)(2,1)}) %all-gather.4.cloned.1.call-update) | async-done | bytes 2097168 | tf_op jit(solution)/shard_map/all_gather | solution.py:94
  79.5 2.5 multiply_reduce_fusion.3
  82.7 2.5 fusion.22
  86.8 3.0 %multiply_cosine_fusion.1 = (f32[512,32]{1,0:T(8,128)S(1)}, f32[512,32]{1,0:T(8,128)}, f32[512,32]{1,0:T(8,128)}, f32[512,32]{1,0:T(8,128)}) fusion(f32[32]{0:T(128)S(1)} %multiply_power_fusion, f32[512]{0:T(512)S(1)} %get-tuple-element.112, f32[512]{0:T(512)S(1)} %get-tuple-element.113), kind=kLoop, calls=%fused_computation.50 | loop fusion | flops 32768 | bytes 266368 | tf_op jit(solution)/shard_map/cos | solution.py:40
  92.6 40.4 %all_gather.17 = bf16[512,2,128]{2,0,1:T(8,128)(2,1)} all-gather(bf16[16,2,128]{2,0,1:T(8,128)(2,1)S(1)} %pad_maximum_fusion.2), channel_id=1, replica_groups=mesh['sp_0'=8,'sp_1'=4,'tp'=8] {'sp_0','sp_1'}, dimensions={0}, use_global_device_ids=true | all-gather | bytes 270336 | tf_op jit(solution)/shard_map/all_gather | solution.py:23
  139.6 46.4 %all-gather.6.cloned.1.call-done = bf16[16384,2,128]{0,2,1:T(8,128)(2,1)} async-done(((bf16[512,2,128]{0,2,1:T(8,128)(2,1)}), bf16[16384,2,128]{0,2,1:T(8,128)(2,1)}) %all-gather.6.cloned.1.call-update) | async-done | bytes 8388624 | tf_op jit(solution)/shard_map/all_gather | solution.py:23
  186.1 5.8 %fusion.76 = (bf16[16384,1,128]{0,2,1:T(8,128)(2,1)}, bf16[16384,1,128]{0,2,1:T(8,128)(2,1)}) fusion(bf16[16384,2,128]{0,2,1:T(8,128)(2,1)} %all-gather.6.cloned.1.call-done), kind=kLoop, calls=%fused_computation.126 | loop fusion | bytes 16777216 | tf_op jit(solution)/shard_map/slice | solution.py:25
  191.9 6.3 %copy.23 = bf16[16384,1,128]{2,0,1:T(8,128)(2,1)} copy(bf16[16384,1,128]{0,2,1:T(8,128)(2,1)} %get-tuple-element.78) | data formatting | bytes 8388608 | tf_op jit(solution)/shard_map/while | solution.py:172
  198.2 6.5 %copy.24 = bf16[16384,1,128]{2,0,1:T(8,128)(2,1)} copy(bf16[16384,1,128]{0,2,1:T(8,128)(2,1)} %get-tuple-element.77) | data formatting | bytes 8388608 | tf_op jit(solution)/shard_map/while | solution.py:172
  204.7 52.6 %while.14 = (s32[]{:T(128)}, f32[1,1024]{1,0:T(1,128)S(1)}, f32[1,1024]{1,0:T(1,128)S(1)}, f32[1,1024,128]{2,1,0:T(8,128)S(1)}, bf16[8,2048,1,128]{3,1,2,0:T(8,1...) while((s32[]{:T(128)}, f32[1,1024]{1,0:T(1,128)S(1)}, ...), condition=%wide.region_12.13_spmd, body=%wide.region_9.12_spmd.sunk | while | flops 1090783232 | bytes 27590756 | solution.py:172
  204.7 2.3 multiply_reduce_fusion.6
  208.5 2.8 fusion.97
  215.1 2.8 fusion.97
  221.6 2.8 fusion.97
  228.2 2.8 fusion.97
  234.8 2.8 fusion.97
  241.4 2.8 fusion.97
  247.9 2.8 fusion.97
  254.5 2.8 fusion.97
  258.0 14.5 %all_to_all.19 = bf16[8,64,256]{2,1,0:T(8,128)(2,1)S(1)} all-to-all(bf16[8,64,256]{2,1,0:T(8,128)(2,1)S(1)} %all_to_all.14), channel_id=1, replica_groups=mesh['sp_0'=8,'sp_1'=4,'tp'=8] {'tp'}, dimensions={0} | all-to-all | bytes 524288 | tf_op jit(solution)/shard_map/all_to_all | solution.py:180
  272.5 5.1 %multiply_reduce_fusion.1 = (f32[64]{0:T(128)S(1)}, f32[64,2048]{1,0:T(8,128)S(1)}) fusion(bf16[64,2048]{1,0:T(8,128)(2,1)S(1)} %bitcast.110, bf16[2048,2048]{1,0:T(8,128)(2,1)} %all-gather.8.cloned.1.call-done), kind=kOutput, calls=%fused_computation.39 | convolution fusion | flops 537132992 | bytes 9175296 | tf_op jit(solution)/shard_map/dot_general | solution.py:181
  (93 shorter events, 45.2 us)
Async XLA Ops:
  6.5 126.6 %copy-start = (bf16[2048,256]{1,0:T(8,128)(2,1)S(1)}, bf16[2048,256]{1,0:T(8,128)(2,1)}, u32[]{:S(2)}) copy-start(bf16[2048,256]{1,0:T(8,128)(2,1)} %param.18) | copy-start | bytes 3145732
  6.5 75.5 %copy-start.5 = (f32[128]{0:T(128)S(1)}, f32[128]{0:T(128)}, u32[]{:S(2)}) copy-start(f32[128]{0:T(128)} %param.23) | copy-start | bytes 1540
  6.5 73.0 %all-gather.4.cloned.1.call-start = ((), (), s32[]{:S(2)}) async-start(), calls=%async_computation.1 | async-start | bytes 2359296 | tf_op jit(solution)/shard_map/all_gather | solution.py:94
  56.4 129.7 %all-gather.6.cloned.1.call-start = ((), (), s32[]{:S(2)}) async-start(), calls=%async_computation.2 | async-start | bytes 8650752 | tf_op jit(solution)/shard_map/all_gather | solution.py:23
  56.4 33.3 %copy-start.4 = (bf16[16,2048]{1,0:T(8,128)(2,1)S(1)}, bf16[16,2048]{1,0:T(8,128)(2,1)}, u32[]{:S(2)}) copy-start(bf16[16,2048]{1,0:T(8,128)(2,1)} %param.14) | copy-start | bytes 196612
  82.1 51.0 %copy-start.1 = (bf16[512,2048]{1,0:T(8,128)(2,1)S(1)}, bf16[512,2048]{1,0:T(8,128)(2,1)}, u32[]{:S(2)}) copy-start(bf16[512,2048]{1,0:T(8,128)(2,1)} %all-gather.4.cloned.1.call-done) | copy-start | bytes 6291460
  86.0 49.9 %copy-start.6 = (f32[128]{0:T(128)S(1)}, f32[128]{0:T(128)}, u32[]{:S(2)}) copy-start(f32[128]{0:T(128)} %param.22) | copy-start | bytes 1540
  86.0 186.5 %all-gather.8.cloned.1.call-start = ((), (), s32[]{:S(2)}) async-start(), calls=%async_computation.3 | async-start | bytes 9437184 | tf_op jit(solution)/shard_map/all_gather | solution.py:183
  134.7 3.5 %copy-start.3 = (bf16[512,2,128]{2,0,1:T(8,128)(2,1)S(1)}, bf16[512,2,128]{2,0,1:T(8,128)(2,1)}, u32[]{:S(2)}) copy-start(bf16[512,2,128]{2,0,1:T(8,128)(2,1)} %all_gather.17) | copy-start | bytes 786436
  272.5 5.1 %copy-start.2 = (bf16[64,2048]{1,0:T(8,128)(2,1)S(1)}, bf16[64,2048]{1,0:T(8,128)(2,1)}, u32[]{:S(2)}) copy-start(bf16[64,2048]{1,0:T(8,128)(2,1)} %param.13) | copy-start | bytes 786436
Sparse Core Ops, SparseCore 0:
  56.5 23.0 all-gather.3
  86.1 99.8 all-gather.5
  187.9 54.6 all-gather.7
where the time goes:
time: 286 us; the launch traced here: 285 us
  blocking collectives  100 us (35%)
  waiting for transfers between devices  70.3 us (25%)
  matrix products  57.2 us (20%)
  other arithmetic  22.9 us (8%)
  local copies, waits for them, and re-layouts  20.4 us (7%)
  between operations  13.4 us (5%)
    all_gather x1, waiting for transfers between devices, side_by_side(): filled, at, done = (lax.all_gather(both, axis, axis=dim, tiled=True), 0, [])  46.4 us
    all_gather x1, blocking collectives, side_by_side(): filled, at, done = (lax.all_gather(both, axis, axis=dim, tiled=True), 0, [])  40.4 us
    psum x2, blocking collectives, over_axes(): value = lax.psum(value, axis)  26.1 us
    all_gather x1, waiting for transfers between devices, body(): piece = lax.all_gather(normalised_rows, 'tp', axis=0, tiled=True)  23.1 us
    dot_general x8, matrix products, update(): jnp.einsum('hqk,khd->hqd', weights_now.astype(jnp.bfloat16), value_block,...  22.2 us
    all_gather x1, blocking collectives, body(): modulation = lax.all_gather(summed, 'tp', axis=1, tiled=True)  19.5 us
    dot_general x8, matrix products, update(): jnp.einsum('hqd,khd->hqk', grouped, key_block, preferred_element_type=jnp...  18.4 us
    all_to_all x1, blocking collectives, body(): lax.all_to_all(attended, 'tp', split_axis=0, concat_axis=1, tiled=True)  14.5 us
  transfers between devices with their start and end apart: 3, of which 2 were waited for; matrix products, arithmetic and copies ran while one was open for 29% of the time, Pallas kernels for 0%

commit v1 on v0

--- a/solution.py
+++ b/solution.py
@@ -91,7 +91,8 @@
     prefix_normalised = modulate(context, modulation[1])
     query_cols = query_weight.shape[1]
     key_cols = key_matrix.shape[1]
-    piece = lax.all_gather(normalised_rows, "tp", axis=0, tiled=True)
+    outgoing = jnp.stack([normalised_rows] * lax.axis_size("tp"))
+    piece = jnp.concatenate(lax.all_to_all(outgoing, "tp", 0, 0), axis=0)
     projected = jnp.concatenate(
         [
             jnp.dot(piece, query_weight, preferred_element_type=jnp.float32),

time: 286 us -> 285 us (level)
  waiting for transfers between devices: 70.3 us -> 80.3 us
  blocking collectives: 100 us -> 92.4 us
  other arithmetic: 22.9 us -> 17.8 us
  matrix products: 57.2 us -> 52.2 us
  starting transfers between devices: 0.09 us -> 4.1 us
    all_to_all x0 -> x1, waiting for transfers between devices: none -> 26.2 us  [body(): piece = jnp.concatenate(lax.all_to_all(outgoing, 'tp', 0, 0), axis=0)]
    all_gather x1 -> x0, waiting for transfers between devices: 23.1 us -> none  [body(): piece = lax.all_gather(normalised_rows, 'tp', axis=0, tiled=True)]
    all_gather x1, blocking collectives: 40.4 us -> 32.4 us  [side_by_side(): filled, at, done = (lax.all_gather(both, axis, axis=dim, tiled=True), 0, [])]
    all_gather x1, waiting for transfers between devices: 46.4 us -> 53.4 us  [side_by_side(): filled, at, done = (lax.all_gather(both, axis, axis=dim, tiled=True), 0, [])]
    all_to_all x0 -> x1, starting transfers between devices: none -> 4.06 us  [body(): piece = jnp.concatenate(lax.all_to_all(outgoing, 'tp', 0, 0), axis=0)]
  transfers between devices with their start and end apart: 3 -> 3, of which waited for: 2 -> 2; matrix products, arithmetic and copies ran while one was open for 29% -> 28% of each run, Pallas kernels for 0% -> 0%
where the time goes in v1:
time: 285 us; the launch traced here: 284 us
  blocking collectives  92.4 us (32%)
  waiting for transfers between devices  80.3 us (28%)
  matrix products  52.2 us (18%)
  local copies, waits for them, and re-layouts  23.2 us (8%)
  other arithmetic  17.8 us (6%)
  between operations  13.6 us (5%)
  starting transfers between devices  4.1 us (1%)
    all_gather x1, waiting for transfers between devices, side_by_side(): filled, at, done = (lax.all_gather(both, axis, axis=dim, tiled=True), 0, [])  53.4 us
    all_gather x1, blocking collectives, side_by_side(): filled, at, done = (lax.all_gather(both, axis, axis=dim, tiled=True), 0, [])  32.4 us
    all_to_all x1, waiting for transfers between devices, body(): piece = jnp.concatenate(lax.all_to_all(outgoing, 'tp', 0, 0), axis=0)  26.2 us
    psum x2, blocking collectives, over_axes(): value = lax.psum(value, axis)  26.1 us
    dot_general x8, matrix products, update(): jnp.einsum('hqk,khd->hqd', weights_now.astype(jnp.bfloat16), value_block,...  22.2 us
    all_gather x1, blocking collectives, body(): modulation = lax.all_gather(summed, 'tp', axis=1, tiled=True)  19.5 us
    dot_general x8, matrix products, update(): jnp.einsum('hqd,khd->hqk', grouped, key_block, preferred_element_type=jnp...  18.4 us
    all_to_all x1, blocking collectives, body(): lax.all_to_all(attended, 'tp', split_axis=0, concat_axis=1, tiled=True)  14.5 us
  transfers between devices with their start and end apart: 3, of which 2 were waited for; matrix products, arithmetic and copies ran while one was open for 28% of the time, Pallas kernels for 0%

profile of v1, /device:TPU:1, one launch (start us, length us, event | category | flops | bytes accessed | tf_op | source)
XLA Modules:
  0.0 284.0 jit_solution(8890586815705257067)
XLA Ops:
  7.8 17.5 %psum.14 = f32[2,768]{1,0:T(2,128)S(1)} all-reduce(f32[2,768]{1,0:T(2,128)S(1)} %fusion.67), channel_id=1, replica_groups=mesh['sp_0'=8,'sp_1'=4,'tp'=8] {'sp_0'}, use_global_device_ids=true, to_apply=%region_0.1 | all-reduce | flops 1536 | bytes 12288 | tf_op jit(solution)/shard_map/psum | solution.py:17
  25.3 8.6 %psum.15 = f32[2,768]{1,0:T(2,128)S(1)} all-reduce(f32[2,768]{1,0:T(2,128)S(1)} %psum.14), channel_id=1, replica_groups=mesh['sp_0'=8,'sp_1'=4,'tp'=8] {'sp_1'}, use_global_device_ids=true, to_apply=%region_1.2 | all-reduce | flops 1536 | bytes 12288 | tf_op jit(solution)/shard_map/psum | solution.py:17
  33.9 19.5 %all_gather.12 = f32[2,6144]{1,0:T(2,128)S(1)} all-gather(f32[2,768]{1,0:T(2,128)S(1)} %psum.15), channel_id=1, replica_groups=mesh['sp_0'=8,'sp_1'=4,'tp'=8] {'tp'}, dimensions={1}, use_global_device_ids=true | all-gather | bytes 55296 | tf_op jit(solution)/shard_map/all_gather | solution.py:88
  57.2 4.1 %all-to-all-start = ((bf16[8,64,2048]{2,1,0:T(8,128)(2,1)}), bf16[8,64,2048]{2,1,0:T(8,128)(2,1)S(1)}, u32[]{:S(2)}, u32[]{:S(2)}) async-start(bf16[8,64,2048]{2,1,0:T(8,128)(2,1)} %stack.11), calls=%async_computation | async-start | bytes 4194304 | tf_op jit(solution)/shard_map/all_to_all | solution.py:95
  61.3 26.2 %all-to-all-done = bf16[8,64,2048]{2,1,0:T(8,128)(2,1)S(1)} async-done(((bf16[8,64,2048]{2,1,0:T(8,128)(2,1)}), bf16[8,64,2048]{2,1,0:T(8,128)(2,1)S(1)}, u32[]{:S(2)}, u32[]{:S(2)}) %all-to-all-start) | async-done | bytes 2097184 | tf_op jit(solution)/shard_map/all_to_all | solution.py:95
  95.1 32.4 %all_gather.13 = bf16[512,2,128]{2,0,1:T(8,128)(2,1)S(1)} all-gather(bf16[16,2,128]{2,0,1:T(8,128)(2,1)S(1)} %pad_maximum_fusion.1), channel_id=1, replica_groups=mesh['sp_0'=8,'sp_1'=4,'tp'=8] {'sp_0','sp_1'}, dimensions={0}, use_global_device_ids=true | all-gather | bytes 270336 | tf_op jit(solution)/shard_map/all_gather | solution.py:23
  131.4 53.4 %all-gather.3.cloned.1.call-done = bf16[16384,2,128]{0,2,1:T(8,128)(2,1)} async-done(((bf16[512,2,128]{0,2,1:T(8,128)(2,1)}), bf16[16384,2,128]{0,2,1:T(8,128)(2,1)}) %all-gather.3.cloned.1.call-update) | async-done | bytes 8388624 | tf_op jit(solution)/shard_map/all_gather | solution.py:23
  184.7 5.8 %fusion.76 = (bf16[16384,1,128]{0,2,1:T(8,128)(2,1)}, bf16[16384,1,128]{0,2,1:T(8,128)(2,1)}) fusion(bf16[16384,2,128]{0,2,1:T(8,128)(2,1)} %all-gather.3.cloned.1.call-done), kind=kLoop, calls=%fused_computation.126 | loop fusion | bytes 16777216 | tf_op jit(solution)/shard_map/slice | solution.py:25
  190.5 6.3 %copy.26 = bf16[16384,1,128]{2,0,1:T(8,128)(2,1)} copy(bf16[16384,1,128]{0,2,1:T(8,128)(2,1)} %get-tuple-element.78) | data formatting | bytes 8388608 | tf_op jit(solution)/shard_map/while | solution.py:173
  196.9 6.5 %copy.27 = bf16[16384,1,128]{2,0,1:T(8,128)(2,1)} copy(bf16[16384,1,128]{0,2,1:T(8,128)(2,1)} %get-tuple-element.77) | data formatting | bytes 8388608 | tf_op jit(solution)/shard_map/while | solution.py:173
  203.4 52.6 %while.14 = (s32[]{:T(128)}, f32[1,1024]{1,0:T(1,128)S(1)}, f32[1,1024]{1,0:T(1,128)S(1)}, f32[1,1024,128]{2,1,0:T(8,128)S(1)}, bf16[8,2048,1,128]{3,1,2,0:T(8,1...) while((s32[]{:T(128)}, f32[1,1024]{1,0:T(1,128)S(1)}, ...), condition=%wide.region_12.13_spmd, body=%wide.region_9.12_spmd.sunk | while | flops 1090783232 | bytes 27590756 | solution.py:173
  203.4 2.3 multiply_reduce_fusion.6
  207.2 2.8 fusion.97
  213.7 2.8 fusion.97
  220.3 2.8 fusion.97
  223.1 2.3 multiply_reduce_fusion.6
  226.9 2.8 fusion.97
  233.5 2.8 fusion.97
  236.3 2.3 multiply_reduce_fusion.6
  240.0 2.8 fusion.97
  246.6 2.8 fusion.97
  253.2 2.8 fusion.97
  256.6 14.5 %all_to_all.24 = bf16[8,64,256]{2,1,0:T(8,128)(2,1)S(1)} all-to-all(bf16[8,64,256]{2,1,0:T(8,128)(2,1)S(1)} %all_to_all.18), channel_id=1, replica_groups=mesh['sp_0'=8,'sp_1'=4,'tp'=8] {'tp'}, dimensions={0} | all-to-all | bytes 524288 | tf_op jit(solution)/shard_map/all_to_all | solution.py:181
  271.2 5.1 %multiply_reduce_fusion.1 = (f32[64]{0:T(128)S(1)}, f32[64,2048]{1,0:T(8,128)S(1)}) fusion(bf16[64,2048]{1,0:T(8,128)(2,1)S(1)} %bitcast.115, bf16[2048,2048]{1,0:T(8,128)(2,1)} %all-gather.5.cloned.1.call-done), kind=kOutput, calls=%fused_computation.39 | convolution fusion | flops 537132992 | bytes 9175296 | tf_op jit(solution)/shard_map/dot_general | solution.py:182
  (92 shorter events, 41.2 us)
Async XLA Ops:
  6.5 81.8 %copy-start = (bf16[2048,128]{1,0:T(8,128)(2,1)S(1)}, bf16[2048,128]{1,0:T(8,128)(2,1)}, u32[]{:S(2)}) copy-start(bf16[2048,128]{1,0:T(8,128)(2,1)} %param.19) | copy-start | bytes 1572868
  6.5 81.0 %copy-start.2 = (bf16[2048,128]{1,0:T(8,128)(2,1)S(1)}, bf16[2048,128]{1,0:T(8,128)(2,1)}, u32[]{:S(2)}) copy-start(bf16[2048,128]{1,0:T(8,128)(2,1)} %param.20) | copy-start | bytes 1572868
  57.2 32.0 %copy-start.4 = (f32[128]{0:T(128)S(1)}, f32[128]{0:T(128)}, u32[]{:S(2)}) copy-start(f32[128]{0:T(128)} %param.23) | copy-start | bytes 1540
  57.2 30.3 %all-to-all-start = ((bf16[8,64,2048]{2,1,0:T(8,128)(2,1)}), bf16[8,64,2048]{2,1,0:T(8,128)(2,1)S(1)}, u32[]{:S(2)}, u32[]{:S(2)}) async-start(bf16[8,64,2048]{2,1,0:T(8,128)(2,1)} %stack.11), calls=%async_computation | async-start | bytes 4194304 | tf_op jit(solution)/shard_map/all_to_all | solution.py:95
  61.3 123.4 %all-gather.3.cloned.1.call-start = ((), (), s32[]{:S(2)}) async-start(), calls=%async_computation.2 | async-start | bytes 8650752 | tf_op jit(solution)/shard_map/all_gather | solution.py:23
  87.5 4.4 %copy-start.3 = (bf16[16,2048]{1,0:T(8,128)(2,1)S(1)}, bf16[16,2048]{1,0:T(8,128)(2,1)}, u32[]{:S(2)}) copy-start(bf16[16,2048]{1,0:T(8,128)(2,1)} %param.14) | copy-start | bytes 196612
  90.6 180.5 %all-gather.5.cloned.1.call-start = ((), (), s32[]{:S(2)}) async-start(), calls=%async_computation.3 | async-start | bytes 9437184 | tf_op jit(solution)/shard_map/all_gather | solution.py:184
  91.9 37.5 %copy-start.5 = (f32[128]{0:T(128)S(1)}, f32[128]{0:T(128)}, u32[]{:S(2)}) copy-start(f32[128]{0:T(128)} %param.22) | copy-start | bytes 1540
  271.2 5.1 %copy-start.1 = (bf16[64,2048]{1,0:T(8,128)(2,1)S(1)}, bf16[64,2048]{1,0:T(8,128)(2,1)}, u32[]{:S(2)}) copy-start(bf16[64,2048]{1,0:T(8,128)(2,1)} %param.13) | copy-start | bytes 786436
Sparse Core Ops, SparseCore 0:
  90.7 93.9 all-gather.2
  186.6 54.6 all-gather.4
